TPU v7x, 32 devices: a whole 2x2x4 slice. The times are simulated.
32 devices in a mesh: sp: 8 (over z, y), tp: 4 (over x, core).
Axes of the slice: x: 2, y: 2, z: 4, core: 2. Of those that a mesh axis runs over, the one named last changes fastest.
Arguments:
- tokens: bfloat16 [8192, 2048], P('sp', 'tp'), may hold values from -600 to 600, as said below
- norm_gain: float32 [2048], replicated, may hold values from 0.1 to 1.9
- w_query: bfloat16 [2048, 1024], P(None, 'tp'), may hold values from -0.125 to 0.125
- w_forget_fwd: bfloat16 [2048, 1024], P(None, 'tp'), may hold values from -0.125 to 0.125
- w_forget_bwd: bfloat16 [2048, 1024], P(None, 'tp'), may hold values from -0.125 to 0.125
- w_value: bfloat16 [2048, 1024], P(None, 'tp'), may hold values from -0.125 to 0.125
- w_gate: bfloat16 [2048, 1024], P(None, 'tp'), may hold values from -0.125 to 0.125
- w_pool_in: bfloat16 [2048, 1024], P(None, 'tp'), may hold values from -0.125 to 0.125
- forget_gap: float32 [2, 1024], P(None, 'tp'), may hold values from 0 to 0.06
- added_log_retention: float32 [8192, 8], P('sp', 'tp'), may hold values from -2.1 to 0
- initial_state: float32 [2, 8, 128, 128], P(None, 'tp'), may hold values from -0.18 to 0.18
- head_gain: float32 [1024], P('tp'), may hold values from 0.1 to 1.9
- pool_mix: bfloat16 [4, 256, 256], P('tp'), may hold values from -0.375 to 0.375
- pool_gain: float32 [1024], P('tp'), may hold values from 0.1 to 1.9
- w_out_recur: bfloat16 [1024, 2048], P('tp'), may hold values from -0.125 to 0.125
- w_out_pool: bfloat16 [1024, 2048], P('tp'), may hold values from -0.125 to 0.125
Outputs:
- mixed_out: bfloat16 [8192, 2048], P(('sp', 'tp'))
Inputs may be any that keep to these rules, and one draw needn't show every extreme that they name: `tokens`: layer input with scales that differ between rows and between columns.
All inputs are finite; a program needn't handle non-finite values.
Results may differ from a plain program's by a relative error of at most 0.013.
Values may be sent and summed in bfloat16 or wider, within the bound.
A program may use at most 128 MiB of HBM per device.

v0:
```python
import functools

import jax
import jax.numpy as jnp
from jax import lax
from jax.experimental import pallas as pl
from jax.experimental.pallas import tpu as pltpu
from jax.sharding import PartitionSpec as P

DEPTH = 128
CHUNK = 128
EPSILON = 1e-06
MESH = pl.DeviceIdType.MESH
F32 = jnp.float32
BF16 = jnp.bfloat16
VMEM_LIMIT = 60 * 1024 * 1024
ANY = pl.BlockSpec(memory_space=pl.ANY)
VM = pl.BlockSpec(memory_space=pltpu.VMEM)


def dot(a, b):
    return jnp.dot(a, b, preferred_element_type=F32)


def dot_t(a, b):
    return lax.dot_general(a, b, (((1,), (1,)), ((), ())), preferred_element_type=F32)


def t_dot(a, b, precision=None):
    return lax.dot_general(
        a, b, (((0,), (0,)), ((), ())), preferred_element_type=F32, precision=precision
    )


def peers():
    me = lax.axis_index("tp")
    sibling = me + 1 - 2 * lax.rem(me, 2)
    across = lax.rem(me + 2, 4)
    return me, sibling, across, lax.rem(sibling + 2, 4)


def greet(*devices):
    barrier = pltpu.get_barrier_semaphore()
    for device in devices:
        pl.semaphore_signal(barrier, inc=1, device_id={"tp": device}, device_id_type=MESH)
    pl.semaphore_wait(barrier, len(devices))


def project_kernel(pieces, tokens, gain, *refs):
    weights, outs = refs[:6], refs[6:12]
    held, wide, acc, square, w_sem, sib_sem, x_send, x_recv, f_send, f_recv = refs[12:]
    me, sibling, across, opposite = peers()
    length, width = tokens.shape
    rows = length // pieces
    loads = [pltpu.make_async_copy(w, wide.at[i], w_sem.at[i]) for i, w in enumerate(weights)]
    for load in loads:
        load.start()
    greet(sibling, across)

    def crossing(i):
        at = pl.ds(i * rows, rows)
        return pltpu.make_async_remote_copy(
            tokens.at[at], held.at[1, at], x_send.at[i], x_recv.at[i],
            device_id={"tp": across}, device_id_type=MESH,
        )

    def relay(i):
        at = pl.ds(i * rows, rows)
        return pltpu.make_async_remote_copy(
            held.at[1, at], held.at[2, at], f_send.at[i], f_recv.at[i],
            device_id={"tp": sibling}, device_id_type=MESH,
        )

    beside = pltpu.make_async_remote_copy(
        tokens, held.at[0], sib_sem.at[0], sib_sem.at[1],
        device_id={"tp": sibling}, device_id_type=MESH,
    )
    for i in range(pieces):
        crossing(i).start()
    beside.start()

    def part(block, owner, at, first):
        columns = pl.ds(pl.multiple_of(owner * width, width), width)
        x = block.astype(F32)
        total = jnp.sum(x * x, axis=1, keepdims=True)
        normed = (x * gain[:, columns]).astype(BF16)
        square[at, :] = total if first else square[at, :] + total
        for j in range(6):
            y = dot(normed, wide[j, columns, :])
            acc[j, at, :] = y if first else acc[j, at, :] + y

    for load in loads:
        load.wait()

    def own(i, _):
        at = pl.ds(pl.multiple_of(i * rows, rows), rows)
        part(tokens[at, :], me, at, True)
        return 0

    lax.fori_loop(0, pieces, own, 0)
    beside.wait()

    def near(i, _):
        at = pl.ds(pl.multiple_of(i * rows, rows), rows)
        part(held[0, at, :], sibling, at, False)
        return 0

    lax.fori_loop(0, pieces, near, 0)
    features = width * 4

    def far(i, _):
        at = pl.ds(pl.multiple_of(i * rows, rows), rows)
        crossing(i).wait_recv()
        relay(i).start()
        part(held[1, at, :], across, at, False)
        relay(i).wait_recv()
        part(held[2, at, :], opposite, at, False)
        scale = lax.rsqrt(square[at, :] / features + EPSILON)
        for j in range(6):
            outs[j][at, :] = (acc[j, at, :] * scale).astype(BF16)
        return 0

    lax.fori_loop(0, pieces, far, 0)
    for i in range(pieces):
        crossing(i).wait_send()
        relay(i).wait_send()


def project(tokens, gain, weights):
    length, width = tokens.shape
    depth, columns = weights[0].shape
    pieces = 4
    return pl.pallas_call(
        functools.partial(project_kernel, pieces),
        out_shape=[jax.ShapeDtypeStruct((length, columns), BF16)] * 6,
        in_specs=[VM, VM] + [ANY] * 6,
        out_specs=[VM] * 6,
        scratch_shapes=[
            pltpu.VMEM((3, length, width), BF16),
            pltpu.VMEM((6, depth, columns), BF16),
            pltpu.VMEM((6, length, columns), F32),
            pltpu.VMEM((length, 1), F32),
            pltpu.SemaphoreType.DMA((6,)),
            pltpu.SemaphoreType.DMA((2,)),
            pltpu.SemaphoreType.DMA((pieces,)),
            pltpu.SemaphoreType.DMA((pieces,)),
            pltpu.SemaphoreType.DMA((pieces,)),
            pltpu.SemaphoreType.DMA((pieces,)),
        ],
        compiler_params=pltpu.CompilerParams(
            collective_id=0, has_side_effects=True, vmem_limit_bytes=VMEM_LIMIT
        ),
        name="project",
    )(tokens, gain, *weights)


def strides():
    count = lax.axis_size("sp")
    return [1 << k for k in range(count.bit_length()) if 1 << k < count]


def partner(d, stride):
    me, count = lax.axis_index("sp"), lax.axis_size("sp")
    above, below = me + stride < count, me >= stride
    return (above, me + stride, below) if d == 0 else (below, me - stride, above)


def meet():
    barrier = pltpu.get_barrier_semaphore()
    for stride in strides():
        for d in range(2):
            exists, target, _ = partner(d, stride)

            @pl.when(exists)
            def _():
                pl.semaphore_signal(
                    barrier, inc=1, device_id={"sp": target}, device_id_type=MESH
                )

    number = jnp.int32(0)
    for stride in strides():
        for d in range(2):
            exists, _, _ = partner(d, stride)
            number = number + jnp.where(exists, 1, 0)
    pl.semaphore_wait(barrier, number)


def edge_copy(d, pool_in, edge, e_send, e_recv):
    length, rim = pool_in.shape[0], edge.shape[1]
    _, target, _ = partner(d, 1)
    begin = length - rim if d == 0 else 0
    return pltpu.make_async_remote_copy(
        pool_in.at[pl.ds(begin, rim)], edge.at[d], e_send.at[d], e_recv.at[d],
        device_id={"sp": target}, device_id_type=MESH,
    )


def edges_start(pool_in, edge, e_send, e_recv):
    for d in range(2):
        exists, _, source = partner(d, 1)

        @pl.when(exists)
        def _():
            edge_copy(d, pool_in, edge, e_send, e_recv).start()

        @pl.when(jnp.logical_not(source))
        def _():
            edge[d] = jnp.zeros(edge.shape[1:], edge.dtype)


def edges_close(pool_in, edge, e_send, e_recv):
    for d in range(2):
        exists, _, source = partner(d, 1)

        @pl.when(source)
        def _():
            edge_copy(d, pool_in, edge, e_send, e_recv).wait_recv()

        @pl.when(exists)
        def _():
            edge_copy(d, pool_in, edge, e_send, e_recv).wait_send()


def scan_copy(k, d, stride, sent, landed, p_send, p_recv):
    _, target, _ = partner(d, stride)
    return pltpu.make_async_remote_copy(
        sent.at[k, d], landed.at[k, d], p_send.at[k, d], p_recv.at[k, d],
        device_id={"sp": target}, device_id_type=MESH,
    )


def scan_start(k, state, offset, sent, landed, before, before_keep, p_send, p_recv):
    stride, heads = strides()[k], state.shape[1]
    for d in range(2):
        exists, _, _ = partner(d, stride)

        @pl.when(exists)
        def _():
            for h in range(heads):
                lanes = slice(h * DEPTH, (h + 1) * DEPTH)
                keep = jnp.exp(offset[d, :, lanes])
                sent[k, d, h, :DEPTH, :] = (keep * before[d, h] + state[d, h]).astype(BF16)
                sent[k, d, h, DEPTH:, :] = jnp.broadcast_to(
                    keep * before_keep[d, :, lanes], (16, DEPTH)
                ).astype(BF16)
            scan_copy(k, d, stride, sent, landed, p_send, p_recv).start()


def scan_close(k, state, sent, landed, before, before_keep, p_send, p_recv):
    stride, heads = strides()[k], state.shape[1]
    for d in range(2):
        exists, _, source = partner(d, stride)

        @pl.when(source)
        def _():
            scan_copy(k, d, stride, sent, landed, p_send, p_recv).wait_recv()
            for h in range(heads):
                lanes = slice(h * DEPTH, (h + 1) * DEPTH)
                keep = before_keep[d, :, lanes]
                early = landed[k, d, h].astype(F32)
                before[d, h] = keep * early[:DEPTH] + before[d, h]
                before_keep[d, :, lanes] = keep * early[DEPTH : DEPTH + 1]

        @pl.when(exists)
        def _():
            scan_copy(k, d, stride, sent, landed, p_send, p_recv).wait_send()


def scan_states(state, offset, sent, landed, before, before_keep, p_send, p_recv):
    before[...] = jnp.zeros_like(before)
    before_keep[...] = jnp.ones_like(before_keep)
    for k in range(len(strides())):
        scan_start(k, state, offset, sent, landed, before, before_keep, p_send, p_recv)
        scan_close(k, state, sent, landed, before, before_keep, p_send, p_recv)


def local_kernel(
    query_pre, forget_fwd, forget_bwd, value, gap, added, initial, pool_in,
    out, carried_fwd, carried_bwd, entering, padded,
    state, offset, chunk_state, chunk_keep, sent, landed, before, before_keep, edge,
    p_send, p_recv, e_send, e_recv,
):
    length, width = query_pre.shape
    heads = width // DEPTH
    count = length // CHUNK
    row = lax.broadcasted_iota(jnp.int32, (CHUNK, CHUNK), 0)
    col = lax.broadcasted_iota(jnp.int32, (CHUNK, CHUNK), 1)
    lower = row >= col
    upper = row <= col
    lower_f, upper_f = lower.astype(F32), upper.astype(F32)
    lower_2 = jnp.concatenate([lower_f, lower_f], axis=1).astype(BF16)
    upper_2 = jnp.concatenate([upper_f, upper_f], axis=1).astype(BF16)
    exact = lax.Precision.HIGHEST

    def gates(pre, gap_row, sums):
        enter = gap_row * (1.0 / (1.0 + jnp.exp(pre[...].astype(F32))))
        keep = jnp.log1p(-enter)
        high = keep.astype(BF16)
        low = (keep - high.astype(F32)).astype(BF16)
        return enter, dot(sums, jnp.concatenate([high, low], axis=0))

    meet()
    edges_start(pool_in, edge, e_send, e_recv)
    state[...] = jnp.zeros_like(state)
    offset[...] = jnp.zeros_like(offset)

    def ascend(c, _):
        at = pl.ds(pl.multiple_of(c * CHUNK, CHUNK), CHUNK)
        x = query_pre[at, :].astype(F32)
        query = x / (1.0 + jnp.exp(-x))
        values = value[at, :]
        enter_f, run_f = gates(forget_fwd.at[at], gap[0:1, :], lower_2)
        enter_b, run_b = gates(forget_bwd.at[at], gap[1:2, :], upper_2)
        add = added[at, :]
        col_f = jnp.dot(lower_f, add, precision=exact, preferred_element_type=F32)
        col_b = jnp.dot(upper_f, add, precision=exact, preferred_element_type=F32)
        row_f = t_dot(add, upper_f, exact)
        row_b = t_dot(add, lower_f, exact)
        close_f, close_b = run_f[CHUNK - 1 : CHUNK, :], run_b[0:1, :]
        q_f, q_b = query * jnp.exp(run_f), query * jnp.exp(run_b)
        e_f, e_b = (enter_f * jnp.exp(-run_f)).astype(BF16), (enter_b * jnp.exp(-run_b)).astype(BF16)
        last_f, last_b = enter_f * jnp.exp(close_f - run_f), enter_b * jnp.exp(close_b - run_b)
        for h in range(heads):
            lanes = slice(h * DEPTH, (h + 1) * DEPTH)
            a_col, b_col = col_f[:, h : h + 1], col_b[:, h : h + 1]
            a_row, b_row = row_f[h : h + 1, :], row_b[h : h + 1, :]
            a_end, b_end = a_col[CHUNK - 1 : CHUNK, :], b_col[0:1, :]
            fade_f = jnp.exp(jnp.where(lower, a_col - a_row, -1e30))
            fade_b = jnp.exp(jnp.where(upper, b_col - b_row, -1e30))
            v = values[:, lanes]
            weight = (
                dot_t(q_f[:, lanes].astype(BF16), e_f[:, lanes]) * fade_f
                + dot_t(q_b[:, lanes].astype(BF16), e_b[:, lanes]) * fade_b
            )
            y = dot(weight.astype(BF16), v)
            reach = q_f[:, lanes] * jnp.exp(a_col)
            y = y + dot_t(reach.astype(BF16), state[0, h].astype(BF16))
            out[at, lanes] = y
            carried_fwd[at, lanes] = (reach * jnp.exp(offset[0, :, lanes])).astype(BF16)
            carried_bwd[at, lanes] = (q_b[:, lanes] * jnp.exp(b_col)).astype(BF16)
            total_f = close_f[:, lanes] + a_end
            total_b = close_b[:, lanes] + b_end
            ends_f = (last_f[:, lanes] * jnp.exp(a_end - a_col)).astype(BF16)
            ends_b = (last_b[:, lanes] * jnp.exp(b_end - b_col)).astype(BF16)
            state[0, h] = jnp.exp(total_f) * state[0, h] + t_dot(v, ends_f)
            chunk_state[c, h] = t_dot(v, ends_b)
            chunk_keep[c, :, lanes] = total_b
            offset[0, :, lanes] = offset[0, :, lanes] + total_f
        return 0

    lax.fori_loop(0, count, ascend, 0)

    def descend(i, _):
        c = count - 1 - i
        at = pl.ds(pl.multiple_of(c * CHUNK, CHUNK), CHUNK)
        for h in range(heads):
            lanes = slice(h * DEPTH, (h + 1) * DEPTH)
            reach = carried_bwd[at, lanes]
            out[at, lanes] = out[at, lanes] + dot_t(reach, state[1, h].astype(BF16))
            carried_bwd[at, lanes] = (
                reach.astype(F32) * jnp.exp(offset[1, :, lanes])
            ).astype(BF16)
            total = chunk_keep[c, :, lanes]
            state[1, h] = jnp.exp(total) * state[1, h] + chunk_state[c, h]
            offset[1, :, lanes] = offset[1, :, lanes] + total
        return 0

    lax.fori_loop(0, count, descend, 0)
    scan_states(state, offset, sent, landed, before, before_keep, p_send, p_recv)
    for h in range(heads):
        lanes = slice(h * DEPTH, (h + 1) * DEPTH)
        for d in range(2):
            s = before_keep[d, :, lanes] * initial[d, h].T + before[d, h]
            entering[h, :, d * DEPTH : (d + 1) * DEPTH] = s.astype(BF16)
    rim = edge.shape[1]
    padded[rim : rim + length, :] = pool_in[...]
    edges_close(pool_in, edge, e_send, e_recv)
    padded[:rim, :] = edge[0]
    padded[rim + length :, :] = edge[1]


def local_pass(query_pre, forget_fwd, forget_bwd, value, gap, added, initial, pool_in, rim):
    length, width = query_pre.shape
    heads = width // DEPTH
    count = length // CHUNK
    steps = len(strides())
    flat = jax.ShapeDtypeStruct((length, width), BF16)
    return pl.pallas_call(
        local_kernel,
        out_shape=[
            jax.ShapeDtypeStruct((length, width), F32), flat, flat,
            jax.ShapeDtypeStruct((heads, DEPTH, 2 * DEPTH), BF16),
            jax.ShapeDtypeStruct((length + 2 * rim, pool_in.shape[1]), BF16),
        ],
        in_specs=[VM] * 8,
        out_specs=[VM] * 5,
        scratch_shapes=[
            pltpu.VMEM((2, heads, DEPTH, DEPTH), F32),
            pltpu.VMEM((2, 1, width), F32),
            pltpu.VMEM((count, heads, DEPTH, DEPTH), F32),
            pltpu.VMEM((count, 1, width), F32),
            pltpu.VMEM((steps, 2, heads, DEPTH + 16, DEPTH), BF16),
            pltpu.VMEM((steps, 2, heads, DEPTH + 16, DEPTH), BF16),
            pltpu.VMEM((2, heads, DEPTH, DEPTH), F32),
            pltpu.VMEM((2, 1, width), F32),
            pltpu.VMEM((2, rim, pool_in.shape[1]), BF16),
            pltpu.SemaphoreType.DMA((steps, 2)),
            pltpu.SemaphoreType.DMA((steps, 2)),
            pltpu.SemaphoreType.DMA((2,)),
            pltpu.SemaphoreType.DMA((2,)),
        ],
        compiler_params=pltpu.CompilerParams(
            collective_id=2, has_side_effects=True, vmem_limit_bytes=VMEM_LIMIT
        ),
        name="local",
    )(query_pre, forget_fwd, forget_bwd, value, gap, added, initial, pool_in)


def block_of(begin, rows, refs, scratch, places):
    (local, carried_fwd, carried_bwd, gate_pre, head_gain, padded, mix, pool_gain, w_recur, w_pool) = refs
    entering, = scratch
    rim, sequence, first_row, window = places
    width = local.shape[1]
    heads = width // DEPTH
    at = pl.ds(begin, rows)
    recur = []
    for h in range(heads):
        lanes = slice(h * DEPTH, (h + 1) * DEPTH)
        reach = jnp.concatenate([carried_fwd[at, lanes], carried_bwd[at, lanes]], axis=1)
        both = local[at, lanes] + dot_t(reach, entering[h])
        both = both * lax.rsqrt(jnp.mean(both * both, axis=1, keepdims=True) + EPSILON)
        gate = gate_pre[at, lanes].astype(F32)
        recur.append((both * head_gain[:, lanes] / (1.0 + jnp.exp(-gate))).astype(BF16))
    total = dot(jnp.concatenate(recur, axis=1), w_recur[...])
    span = rows + 2 * rim
    near = padded[pl.ds(begin, span), :]
    target = first_row + begin + lax.broadcasted_iota(jnp.int32, (rows, span), 0)
    source = first_row + begin - rim + lax.broadcasted_iota(jnp.int32, (rows, span), 1)
    low = target - window // 2
    inside = (source >= low) & (source < low + window) & (source >= 0) & (source < sequence)
    start = first_row + begin + lax.broadcasted_iota(jnp.int32, (rows, 1), 0) - window // 2
    number = jnp.minimum(start + window, sequence) - jnp.maximum(start, 0)
    sums = dot(inside.astype(F32).astype(BF16), near)
    mean = sums / number.astype(F32)
    diff = (mean - padded[pl.ds(begin + rim, rows), :].astype(F32)).astype(BF16)
    pooled = (dot(diff, mix[0]) * pool_gain[...]).astype(BF16)
    return total + dot(pooled, w_pool[...])


def finish_kernel(groups, rim, *refs):
    entering, shared, out = refs[0], refs[1:11], refs[11]
    (kept, given, taken, sent, landed, g_send, g_recv, x_send, x_recv) = refs[12:]
    me, sibling, across, opposite = peers()
    greet(sibling, across)
    length = shared[0].shape[0]
    share = length // 4
    rows = kept.shape[1]
    pieces = share // rows
    group = lax.axis_index("tp") * groups
    window = jnp.left_shift(jnp.int32(2), group)
    places = (rim, length * lax.axis_size("sp"), lax.axis_index("sp") * length, window)

    def beside(i):
        return pltpu.make_async_remote_copy(
            given.at[i], taken.at[i], g_send.at[i], g_recv.at[i],
            device_id={"tp": sibling}, device_id_type=MESH,
        )

    def crossing(i):
        return pltpu.make_async_remote_copy(
            sent.at[i], landed.at[i], x_send.at[i], x_recv.at[i],
            device_id={"tp": across}, device_id_type=MESH,
        )

    def partial(owner, p):
        begin = pl.multiple_of(owner * share + p * rows, rows)
        return block_of(begin, rows, shared, (entering,), places).astype(BF16)

    def away(p, _):
        given[p] = partial(opposite, p)
        beside(p).start()
        mine = partial(across, p)
        beside(p).wait_recv()
        sent[p] = (mine.astype(F32) + taken[p].astype(F32)).astype(BF16)
        crossing(p).start()
        return 0

    lax.fori_loop(0, pieces, away, 0)

    def home(p, _):
        given[pieces + p] = partial(sibling, p)
        beside(pieces + p).start()
        kept[p] = partial(me, p)
        return 0

    lax.fori_loop(0, pieces, home, 0)

    def close(p, _):
        beside(pieces + p).wait_recv()
        crossing(p).wait_recv()
        total = kept[p].astype(F32) + taken[pieces + p].astype(F32) + landed[p].astype(F32)
        out[pl.ds(pl.multiple_of(p * rows, rows), rows), :] = total.astype(BF16)
        return 0

    lax.fori_loop(0, pieces, close, 0)
    for i in range(pieces):
        crossing(i).wait_send()
    for i in range(2 * pieces):
        beside(i).wait_send()


def finish(entering, shared, rim):
    length = shared[0].shape[0]
    features = shared[-1].shape[1]
    share, rows = length // 4, 128
    pieces = share // rows
    return pl.pallas_call(
        functools.partial(finish_kernel, shared[6].shape[0], rim),
        out_shape=jax.ShapeDtypeStruct((share, features), BF16),
        in_specs=[VM] * 11,
        out_specs=VM,
        scratch_shapes=[
            pltpu.VMEM((pieces, rows, features), BF16),
            pltpu.VMEM((2 * pieces, rows, features), BF16),
            pltpu.VMEM((2 * pieces, rows, features), BF16),
            pltpu.VMEM((pieces, rows, features), BF16),
            pltpu.VMEM((pieces, rows, features), BF16),
            pltpu.SemaphoreType.DMA((2 * pieces,)),
            pltpu.SemaphoreType.DMA((2 * pieces,)),
            pltpu.SemaphoreType.DMA((pieces,)),
            pltpu.SemaphoreType.DMA((pieces,)),
        ],
        compiler_params=pltpu.CompilerParams(
            collective_id=1, has_side_effects=True, vmem_limit_bytes=VMEM_LIMIT
        ),
        name="finish",
    )(entering, *shared)


def shards(
    tokens, norm_gain, w_query, w_forget_fwd, w_forget_bwd, w_value, w_gate, w_pool_in,
    forget_gap, added_log_retention, initial_state, head_gain, pool_mix, pool_gain,
    w_out_recur, w_out_pool,
):
    weights = (w_query, w_forget_fwd, w_forget_bwd, w_value, w_gate, w_pool_in)
    query_pre, forget_fwd, forget_bwd, value, gate_pre, pool_in = project(
        tokens, norm_gain[None, :], weights
    )
    rim = 16
    local, carried_fwd, carried_bwd, entering, padded = local_pass(
        query_pre, forget_fwd, forget_bwd, value, forget_gap, added_log_retention,
        initial_state, pool_in, rim,
    )
    shared = (
        local, carried_fwd, carried_bwd, gate_pre, head_gain[None, :], padded,
        pool_mix, pool_gain[None, :], w_out_recur, w_out_pool,
    )
    return finish(entering, shared, rim)


def solution(mesh):
    in_specs = (
        P("sp", "tp"), P(), P(None, "tp"), P(None, "tp"), P(None, "tp"), P(None, "tp"),
        P(None, "tp"), P(None, "tp"), P(None, "tp"), P("sp", "tp"), P(None, "tp", None, None),
        P("tp"), P("tp", None, None), P("tp"), P("tp", None), P("tp", None),
    )
    out_specs = P(("sp", "tp"), None)
    return jax.shard_map(shards, mesh=mesh, in_specs=in_specs, out_specs=out_specs, check_vma=False)
```

profile of v0, /device:TPU:0, one launch (start us, length us, event | category | flops | bytes accessed | tf_op | source)
XLA Modules:
  0.0 97.4 jit_solution(17432345215301854867)
XLA Ops:
  0.0 1.7 %copy.17.added = f32[1024,2]{1,0:T(8,128)} copy(f32[1024,2]{0,1:T(2,128)} %param.25) | data formatting | bytes 16384 | tf_op args[9]
  1.7 31.5 %project.1 = (bf16[1024,256]{1,0:T(8,128)(2,1)}, bf16[1024,256]{1,0:T(8,128)(2,1)}, bf16[1024,256]{1,0:T(8,128)(2,1)}, bf16[1024,256]{1,0:T(8,128)(2,1)}, bf16[1...) custom-call(bf16[1024,512]{1,0:T(8,128)(2,1)} %tokens.1, f32[1,2048]{1,0:T(1,128)} %bitcast.3, bf16[2048,256]{1,0:T(8,128)(2,1)} %refs_0_.1, ...), custom_call_target="tpu_custom_call" | custom-call | tf_op jit(solution)/shard_map/project/pallas_call | solution.py:133
  33.2 30.4 %local.1 = (f32[1024,256]{1,0:T(8,128)}, bf16[1024,256]{1,0:T(8,128)(2,1)}, bf16[1024,256]{1,0:T(8,128)(2,1)}, bf16[2,128,256]{2,1,0:T(8,128)(2,1)}, bf16[1056,256]{1,0:T(8,128)(2,1)}) custom-call(bf16[1024,256]{1,0:T(8,128)(2,1)} %get-tuple-element.16.query_pre, bf16[1024,256]{1,0:T(8,128)(2,1)} %get-tuple-element.17.forget_fwd, ...), custom_call_target="tpu_custom_call" | custom-call | tf_op jit(solution)/shard_map/local/pallas_call | solution.py:388
  63.6 31.5 %finish.1 = bf16[256,2048]{1,0:T(8,128)(2,1)} custom-call(bf16[2,128,256]{2,1,0:T(8,128)(2,1)} %get-tuple-element.21.refs_0_, f32[1024,256]{1,0:T(8,128)} %get-tuple-element.22.refs_1_, bf16[1024,256]{1,0:T(8,128)(2,1)} %get-tuple-element.23.refs_2_, bf16[1024,256]{1,0:T(8,128)(2,1)} %get-tuple-element.24.refs_3_, ...), custom_call_target="tpu_custom_call" | custom-call | tf_op jit(solution)/shard_map/finish/pallas_call | solution.py:517
  95.1 2.3 %copy.19 = bf16[256,2048]{1,0:T(8,128)(2,1)} copy(bf16[256,2048]{1,0:T(8,128)(2,1)} %finish.1) | data formatting | bytes 2097152
where the time goes:
time: 97.7 us; the launch traced here: 97.4 us
  Pallas kernels  93.4 us (96%)
  local copies, waits for them, and re-layouts  4.02 us (4%)
    pallas_call x1, Pallas kernels, project(): pl.pallas_call(functools.partial(project_kernel, pieces), out_shape=[jax....  31.5 us
    pallas_call x1, Pallas kernels, finish(): pl.pallas_call(functools.partial(finish_kernel, shared[6].shape[0], rim),...  31.5 us
    pallas_call x1, Pallas kernels, local_pass(): pl.pallas_call(local_kernel, out_shape=[jax.ShapeDtypeStruct((length, wid...  30.4 us
    unnamed x2, local copies, waits for them, and re-layouts  4.02 us

commit v1 on v0

--- a/solution.py
+++ b/solution.py
@@ -266,19 +266,11 @@
             scan_copy(k, d, stride, sent, landed, p_send, p_recv).wait_send()
 
 
-def scan_states(state, offset, sent, landed, before, before_keep, p_send, p_recv):
-    before[...] = jnp.zeros_like(before)
-    before_keep[...] = jnp.ones_like(before_keep)
-    for k in range(len(strides())):
-        scan_start(k, state, offset, sent, landed, before, before_keep, p_send, p_recv)
-        scan_close(k, state, sent, landed, before, before_keep, p_send, p_recv)
-
-
 def local_kernel(
     query_pre, forget_fwd, forget_bwd, value, gap, added, initial, pool_in,
     out, carried_fwd, carried_bwd, entering, padded,
     state, offset, chunk_state, chunk_keep, sent, landed, before, before_keep, edge,
-    p_send, p_recv, e_send, e_recv,
+    p_send, p_recv, e_send, e_recv, enters, runs, cols, starts, offsets,
 ):
     length, width = query_pre.shape
     heads = width // DEPTH
@@ -306,67 +298,86 @@
 
     def ascend(c, _):
         at = pl.ds(pl.multiple_of(c * CHUNK, CHUNK), CHUNK)
-        x = query_pre[at, :].astype(F32)
-        query = x / (1.0 + jnp.exp(-x))
         values = value[at, :]
         enter_f, run_f = gates(forget_fwd.at[at], gap[0:1, :], lower_2)
         enter_b, run_b = gates(forget_bwd.at[at], gap[1:2, :], upper_2)
         add = added[at, :]
         col_f = jnp.dot(lower_f, add, precision=exact, preferred_element_type=F32)
         col_b = jnp.dot(upper_f, add, precision=exact, preferred_element_type=F32)
-        row_f = t_dot(add, upper_f, exact)
-        row_b = t_dot(add, lower_f, exact)
+        enters[0, at, :], enters[1, at, :] = enter_f, enter_b
+        runs[0, at, :], runs[1, at, :] = run_f, run_b
+        cols[0, at, :], cols[1, at, :] = col_f, col_b
         close_f, close_b = run_f[CHUNK - 1 : CHUNK, :], run_b[0:1, :]
-        q_f, q_b = query * jnp.exp(run_f), query * jnp.exp(run_b)
-        e_f, e_b = (enter_f * jnp.exp(-run_f)).astype(BF16), (enter_b * jnp.exp(-run_b)).astype(BF16)
         last_f, last_b = enter_f * jnp.exp(close_f - run_f), enter_b * jnp.exp(close_b - run_b)
+        offsets[0, c] = offset[0]
         for h in range(heads):
             lanes = slice(h * DEPTH, (h + 1) * DEPTH)
             a_col, b_col = col_f[:, h : h + 1], col_b[:, h : h + 1]
-            a_row, b_row = row_f[h : h + 1, :], row_b[h : h + 1, :]
             a_end, b_end = a_col[CHUNK - 1 : CHUNK, :], b_col[0:1, :]
-            fade_f = jnp.exp(jnp.where(lower, a_col - a_row, -1e30))
-            fade_b = jnp.exp(jnp.where(upper, b_col - b_row, -1e30))
             v = values[:, lanes]
+            total_f = close_f[:, lanes] + a_end
+            ends_f = (last_f[:, lanes] * jnp.exp(a_end - a_col)).astype(BF16)
+            ends_b = (last_b[:, lanes] * jnp.exp(b_end - b_col)).astype(BF16)
+            ends = t_dot(v, jnp.concatenate([ends_f, ends_b], axis=1))
+            starts[c, h, :, :DEPTH] = state[0, h].astype(BF16)
+            state[0, h] = jnp.exp(total_f) * state[0, h] + ends[:, :DEPTH]
+            chunk_state[c, h] = ends[:, DEPTH:]
+            chunk_keep[c, :, lanes] = close_b[:, lanes] + b_end
+            offset[0, :, lanes] = offset[0, :, lanes] + total_f
+        return 0
+
+    lax.fori_loop(0, count, ascend, 0)
+
+    def descend(i, _):
+        c = count - 1 - i
+        offsets[1, c] = offset[1]
+        for h in range(heads):
+            lanes = slice(h * DEPTH, (h + 1) * DEPTH)
+            starts[c, h, :, DEPTH:] = state[1, h].astype(BF16)
+            total = chunk_keep[c, :, lanes]
+            state[1, h] = jnp.exp(total) * state[1, h] + chunk_state[c, h]
+            offset[1, :, lanes] = offset[1, :, lanes] + total
+        return 0
+
+    lax.fori_loop(0, count, descend, 0)
+
+    def output(c, _):
+        at = pl.ds(pl.multiple_of(c * CHUNK, CHUNK), CHUNK)
+        x = query_pre[at, :].astype(F32)
+        query = x / (1.0 + jnp.exp(-x))
+        values = value[at, :]
+        run_f, run_b = runs[0, at, :], runs[1, at, :]
+        col_f, col_b = cols[0, at, :], cols[1, at, :]
+        add = added[at, :]
+        row_f = t_dot(add, upper_f, exact)
+        row_b = t_dot(add, lower_f, exact)
+        q_f, q_b = query * jnp.exp(run_f), query * jnp.exp(run_b)
+        e_f = (enters[0, at, :] * jnp.exp(-run_f)).astype(BF16)
+        e_b = (enters[1, at, :] * jnp.exp(-run_b)).astype(BF16)
+        for h in range(heads):
+            lanes = slice(h * DEPTH, (h + 1) * DEPTH)
+            a_col, b_col = col_f[:, h : h + 1], col_b[:, h : h + 1]
+            fade_f = jnp.exp(jnp.where(lower, a_col - row_f[h : h + 1, :], -1e30))
+            fade_b = jnp.exp(jnp.where(upper, b_col - row_b[h : h + 1, :], -1e30))
             weight = (
                 dot_t(q_f[:, lanes].astype(BF16), e_f[:, lanes]) * fade_f
                 + dot_t(q_b[:, lanes].astype(BF16), e_b[:, lanes]) * fade_b
             )
-            y = dot(weight.astype(BF16), v)
-            reach = q_f[:, lanes] * jnp.exp(a_col)
-            y = y + dot_t(reach.astype(BF16), state[0, h].astype(BF16))
-            out[at, lanes] = y
-            carried_fwd[at, lanes] = (reach * jnp.exp(offset[0, :, lanes])).astype(BF16)
-            carried_bwd[at, lanes] = (q_b[:, lanes] * jnp.exp(b_col)).astype(BF16)
-            total_f = close_f[:, lanes] + a_end
-            total_b = close_b[:, lanes] + b_end
-            ends_f = (last_f[:, lanes] * jnp.exp(a_end - a_col)).astype(BF16)
-            ends_b = (last_b[:, lanes] * jnp.exp(b_end - b_col)).astype(BF16)
-            state[0, h] = jnp.exp(total_f) * state[0, h] + t_dot(v, ends_f)
-            chunk_state[c, h] = t_dot(v, ends_b)
-            chunk_keep[c, :, lanes] = total_b
-            offset[0, :, lanes] = offset[0, :, lanes] + total_f
-        return 0
-
-    lax.fori_loop(0, count, ascend, 0)
-
-    def descend(i, _):
-        c = count - 1 - i
-        at = pl.ds(pl.multiple_of(c * CHUNK, CHUNK), CHUNK)
-        for h in range(heads):
-            lanes = slice(h * DEPTH, (h + 1) * DEPTH)
-            reach = carried_bwd[at, lanes]
-            out[at, lanes] = out[at, lanes] + dot_t(reach, state[1, h].astype(BF16))
-            carried_bwd[at, lanes] = (
-                reach.astype(F32) * jnp.exp(offset[1, :, lanes])
-            ).astype(BF16)
-            total = chunk_keep[c, :, lanes]
-            state[1, h] = jnp.exp(total) * state[1, h] + chunk_state[c, h]
-            offset[1, :, lanes] = offset[1, :, lanes] + total
-        return 0
-
-    lax.fori_loop(0, count, descend, 0)
-    scan_states(state, offset, sent, landed, before, before_keep, p_send, p_recv)
+            reach_f = q_f[:, lanes] * jnp.exp(a_col)
+            reach_b = q_b[:, lanes] * jnp.exp(b_col)
+            reach = jnp.concatenate([reach_f, reach_b], axis=1).astype(BF16)
+            out[at, lanes] = dot(weight.astype(BF16), values[:, lanes]) + dot_t(reach, starts[c, h])
+            carried_fwd[at, lanes] = (reach_f * jnp.exp(offsets[0, c, :, lanes])).astype(BF16)
+            carried_bwd[at, lanes] = (reach_b * jnp.exp(offsets[1, c, :, lanes])).astype(BF16)
+        return 0
+
+    before[...] = jnp.zeros_like(before)
+    before_keep[...] = jnp.ones_like(before_keep)
+    steps = len(strides())
+    for k in range(steps):
+        scan_start(k, state, offset, sent, landed, before, before_keep, p_send, p_recv)
+        lax.fori_loop(k * count // steps, (k + 1) * count // steps, output, 0)
+        scan_close(k, state, sent, landed, before, before_keep, p_send, p_recv)
     for h in range(heads):
         lanes = slice(h * DEPTH, (h + 1) * DEPTH)
         for d in range(2):
@@ -408,6 +419,11 @@
             pltpu.SemaphoreType.DMA((steps, 2)),
             pltpu.SemaphoreType.DMA((2,)),
             pltpu.SemaphoreType.DMA((2,)),
+            pltpu.VMEM((2, length, width), F32),
+            pltpu.VMEM((2, length, width), F32),
+            pltpu.VMEM((2, length, heads), F32),
+            pltpu.VMEM((count, heads, DEPTH, 2 * DEPTH), BF16),
+            pltpu.VMEM((2, count, 1, width), F32),
         ],
         compiler_params=pltpu.CompilerParams(
             collective_id=2, has_side_effects=True, vmem_limit_bytes=VMEM_LIMIT

time: 97.7 us -> 95.1 us (0.973)
  Pallas kernels: 93.4 us -> 90.8 us
    pallas_call x1, Pallas kernels: 30.4 us -> 27.8 us  [local_pass(): pl.pallas_call(local_kernel, out_shape=[jax.ShapeDtypeStruct((length, wid...]
where the time goes in v1:
time: 95.1 us; the launch traced here: 94.9 us
  Pallas kernels  90.8 us (95%)
  local copies, waits for them, and re-layouts  4.02 us (4%)
    pallas_call x1, Pallas kernels, project(): pl.pallas_call(functools.partial(project_kernel, pieces), out_shape=[jax....  31.5 us
    pallas_call x1, Pallas kernels, finish(): pl.pallas_call(functools.partial(finish_kernel, shared[6].shape[0], rim),...  31.5 us
    pallas_call x1, Pallas kernels, local_pass(): pl.pallas_call(local_kernel, out_shape=[jax.ShapeDtypeStruct((length, wid...  27.8 us
    unnamed x2, local copies, waits for them, and re-layouts  4.02 us

profile of v1, /device:TPU:0, one launch (start us, length us, event | category | flops | bytes accessed | tf_op | source)
XLA Modules:
  0.0 94.9 jit_solution(2168593264794212377)
XLA Ops:
  0.0 1.7 %copy.17.added = f32[1024,2]{1,0:T(8,128)} copy(f32[1024,2]{0,1:T(2,128)} %param.25) | data formatting | bytes 16384 | tf_op args[9]
  1.7 31.5 %project.1 = (bf16[1024,256]{1,0:T(8,128)(2,1)}, bf16[1024,256]{1,0:T(8,128)(2,1)}, bf16[1024,256]{1,0:T(8,128)(2,1)}, bf16[1024,256]{1,0:T(8,128)(2,1)}, bf16[1...) custom-call(bf16[1024,512]{1,0:T(8,128)(2,1)} %tokens.1, f32[1,2048]{1,0:T(1,128)} %bitcast.3, bf16[2048,256]{1,0:T(8,128)(2,1)} %refs_0_.1, ...), custom_call_target="tpu_custom_call" | custom-call | tf_op jit(solution)/shard_map/project/pallas_call | solution.py:133
  33.2 27.8 %local.1 = (f32[1024,256]{1,0:T(8,128)}, bf16[1024,256]{1,0:T(8,128)(2,1)}, bf16[1024,256]{1,0:T(8,128)(2,1)}, bf16[2,128,256]{2,1,0:T(8,128)(2,1)}, bf16[1056,256]{1,0:T(8,128)(2,1)}) custom-call(bf16[1024,256]{1,0:T(8,128)(2,1)} %get-tuple-element.16.query_pre, bf16[1024,256]{1,0:T(8,128)(2,1)} %get-tuple-element.17.forget_fwd, ...), custom_call_target="tpu_custom_call" | custom-call | tf_op jit(solution)/shard_map/local/pallas_call | solution.py:399
  61.0 31.5 %finish.1 = bf16[256,2048]{1,0:T(8,128)(2,1)} custom-call(bf16[2,128,256]{2,1,0:T(8,128)(2,1)} %get-tuple-element.21.refs_0_, f32[1024,256]{1,0:T(8,128)} %get-tuple-element.22.refs_1_, bf16[1024,256]{1,0:T(8,128)(2,1)} %get-tuple-element.23.refs_2_, bf16[1024,256]{1,0:T(8,128)(2,1)} %get-tuple-element.24.refs_3_, ...), custom_call_target="tpu_custom_call" | custom-call | tf_op jit(solution)/shard_map/finish/pallas_call | solution.py:533
  92.5 2.3 %copy.19 = bf16[256,2048]{1,0:T(8,128)(2,1)} copy(bf16[256,2048]{1,0:T(8,128)(2,1)} %finish.1) | data formatting | bytes 2097152
